TPU v7x, 32 devices: a whole 2x2x4 slice. The times are simulated.
32 devices in a mesh: sp: 8 (over z, y), tp: 4 (over x, core).
Axes of the slice: x: 2, y: 2, z: 4, core: 2. Of those that a mesh axis runs over, the one named last changes fastest.
Arguments:
- resid: bfloat16 [2048, 2048], P(('sp', 'tp')), may hold values from -6 to 6
- mix_in: bfloat16 [2048, 512], P('sp', 'tp'), may hold values from -6 to 6
- decay_rate: float32 [32, 64], P('tp'), may hold values from -0.05 to 0, as said below
- turn_rate: float32 [32, 64], P('tp'), may hold values from -3.140625 to 3.140625
- forget: float32 [2048, 32], P('sp', 'tp'), may hold values from -2 to 0, as said below
- input_real: float32 [32, 64, 16], P('tp'), may hold values from -1 to 1
- input_imag: float32 [32, 64, 16], P('tp'), may hold values from -1 to 1
- output_real: float32 [32, 16, 64], P('tp'), may hold values from -0.75 to 0.75
- output_imag: float32 [32, 16, 64], P('tp'), may hold values from -0.75 to 0.75
- skip_gain: float32 [32, 16], P('tp'), may hold values from -5 to 5
- mix_gain: float32 [512], replicated, may hold values from 0.1 to 1.9
- w_out: bfloat16 [512, 2048], replicated, may hold values from -0.25 to 0.25
- ffn_gain: float32 [2048], replicated, may hold values from 0.1 to 1.9
- gating_matrix: bfloat16 [2048, 5632], P('sp', 'tp'), may hold values from -0.125 to 0.125
- w_up: bfloat16 [2048, 5632], P('sp', 'tp'), may hold values from -0.125 to 0.125
- w_down: bfloat16 [5632, 2048], P('tp', 'sp'), may hold values from -0.078125 to 0.078125
Outputs:
- result: bfloat16 [2048, 2048], P(('sp', 'tp'))
Inputs may be any that keep to these rules, and one draw needn't show every extreme that they name: `decay_rate`: every entry is negative. `forget`: every entry is at most zero.
All inputs are finite; a program needn't handle non-finite values.
Results may differ from a plain program's by a relative error of at most 0.012.
Values may be sent and summed in bfloat16 or wider, within the bound.
A program may use at most 128 MiB of HBM per device.

v0:
```python
import jax
import jax.numpy as jnp
from jax import lax
from jax.sharding import PartitionSpec as P

eps = 1e-06


def carried_in(part, axis, combine, identity):
    place = lax.axis_index(axis)
    gathered = jax.tree.map(lambda a: lax.all_gather(a, axis), part)
    state = jax.tree.map(lambda a, e: jnp.zeros_like(a) + jnp.asarray(e, a.dtype), part, identity)

    def one(turn, state):
        return combine(
            state, jax.tree.map(lambda a: lax.dynamic_index_in_dim(a, turn, 0, False), gathered)
        )

    return lax.fori_loop(0, place, one, state)


def chain(earlier, later):
    first_real, first_imag, push_real, push_imag = earlier
    next_real, next_imag, add_real, add_imag = later
    return (
        next_real * first_real - next_imag * first_imag,
        next_real * first_imag + next_imag * first_real,
        next_real * push_real - next_imag * push_imag + add_real,
        next_real * push_imag + next_imag * push_real + add_imag,
    )


def local_states(log_step, push_real, push_imag, turn):
    high = lax.Precision.HIGHEST
    n_rows, columns = log_step.shape
    span = min(32, n_rows)
    n_spans = n_rows // span
    place = jnp.arange(span, dtype=jnp.float32)
    lower = place[:, None] >= place[None, :]
    lower_cube = lower[:, :, None]
    triangle = lower.astype(jnp.float32)
    lag_angle = (place[:, None] - place[None, :])[:, :, None] * turn[None, None, :]
    lag_cos = jnp.where(lower_cube, jnp.cos(lag_angle), 0.0)
    lag_sin = jnp.where(lower_cube, jnp.sin(lag_angle), 0.0)
    ahead = place + 1.0
    own_cos = jnp.cos(ahead[:, None] * turn[None, :])
    own_sin = jnp.sin(ahead[:, None] * turn[None, :])

    def advance(carry, blocks):
        run_log, state_real, state_imag, offset = carry
        log_block, real_block, imag_block = blocks
        inner = jnp.dot(triangle, log_block, precision=high)
        spread = jnp.where(lower_cube, inner[:, None, :] - inner[None, :, :], 0.0)
        weight = jnp.where(lower_cube, jnp.exp(spread), 0.0)
        weight_real = weight * lag_cos
        weight_imag = weight * lag_sin
        new_real = jnp.sum(weight_real * real_block[None] - weight_imag * imag_block[None], axis=1)
        new_imag = jnp.sum(weight_real * imag_block[None] + weight_imag * real_block[None], axis=1)
        fade = jnp.exp(inner)
        carry_real = fade * own_cos
        carry_imag = fade * own_sin
        new_real = new_real + carry_real * state_real[None] - carry_imag * state_imag[None]
        new_imag = new_imag + carry_real * state_imag[None] + carry_imag * state_real[None]
        whole_fade = jnp.exp(run_log[None] + inner)
        whole_angle = (offset + ahead)[:, None] * turn[None, :]
        prefix_real = whole_fade * jnp.cos(whole_angle)
        prefix_imag = whole_fade * jnp.sin(whole_angle)
        following = (run_log + inner[-1], new_real[-1], new_imag[-1], offset + span)
        return (following, (new_real, new_imag, prefix_real, prefix_imag))

    zero_row = jnp.zeros((columns,), jnp.float32)
    start = (zero_row, zero_row, zero_row, jnp.zeros((), jnp.float32))
    blocks = (
        log_step.reshape(n_spans, span, columns),
        push_real.reshape(n_spans, span, columns),
        push_imag.reshape(n_spans, span, columns),
    )
    final, outputs = lax.scan(advance, start, blocks)
    outputs = tuple((item.reshape(n_rows, columns) for item in outputs))
    total_fade = jnp.exp(final[0])
    totals = (
        total_fade * jnp.cos(n_rows * turn),
        total_fade * jnp.sin(n_rows * turn),
        final[1],
        final[2],
    )
    return (outputs, totals)


def per_device(
    resid,
    mix_in,
    decay_rate,
    turn_rate,
    forget,
    input_real,
    input_imag,
    output_real,
    output_imag,
    skip_gain,
    mix_gain,
    w_out,
    ffn_gain,
    gating_matrix,
    w_up,
    w_down,
):
    high = lax.Precision.HIGHEST
    n_rows, local_width = mix_in.shape
    n_groups, n_state = decay_rate.shape
    n_chan = input_real.shape[2]
    drive = mix_in.astype(jnp.float32).reshape(n_rows, n_groups, n_chan)
    in_factor = jnp.sqrt(-jnp.expm1(2.0 * decay_rate))
    push_real = jnp.einsum(
        "gph,tgh->tgp", input_real * in_factor[:, :, None], drive, precision=high
    ).reshape(n_rows, n_groups * n_state)
    push_imag = jnp.einsum(
        "gph,tgh->tgp", input_imag * in_factor[:, :, None], drive, precision=high
    ).reshape(n_rows, n_groups * n_state)
    log_step = (decay_rate[None] + forget[:, :, None]).reshape(n_rows, n_groups * n_state)
    turn = turn_rate.reshape(n_groups * n_state)
    outputs, totals = local_states(log_step, push_real, push_imag, turn)
    inner_real, inner_imag, prefix_real, prefix_imag = outputs
    ones_row = jnp.ones((n_groups * n_state,), jnp.float32)
    zeroed_row = jnp.zeros((n_groups * n_state,), jnp.float32)
    carry_in = carried_in(totals, "sp", chain, (ones_row, zeroed_row, zeroed_row, zeroed_row))
    state_real = inner_real + prefix_real * carry_in[2][None] - prefix_imag * carry_in[3][None]
    state_imag = inner_imag + prefix_real * carry_in[3][None] + prefix_imag * carry_in[2][None]
    response = (
        jnp.einsum(
            "ghp,tgp->tgh",
            output_real,
            state_real.reshape(n_rows, n_groups, n_state),
            precision=high,
        )
        - jnp.einsum(
            "ghp,tgp->tgh",
            output_imag,
            state_imag.reshape(n_rows, n_groups, n_state),
            precision=high,
        )
        + skip_gain[None] * drive
    )
    mixer_out = jax.nn.gelu(response.reshape(n_rows, local_width)).astype(jnp.bfloat16)
    swapped = lax.all_to_all(mixer_out, "tp", split_axis=0, concat_axis=1, tiled=True)
    mixed_f = swapped.astype(jnp.float32)
    normed = (
        mixed_f * lax.rsqrt(jnp.mean(mixed_f * mixed_f, axis=1, keepdims=True) + eps) * mix_gain
    ).astype(jnp.bfloat16)
    projected = jnp.dot(normed, w_out, preferred_element_type=jnp.float32)
    resid_mid = resid.astype(jnp.float32) + projected
    ffn_in = (
        resid_mid
        * lax.rsqrt(jnp.mean(resid_mid * resid_mid, axis=1, keepdims=True) + eps)
        * ffn_gain
    ).astype(jnp.bfloat16)
    gathered = lax.all_gather(ffn_in, "tp", axis=0, tiled=True)
    gate_val = jnp.dot(
        gathered,
        lax.all_gather(gating_matrix, "sp", axis=0, tiled=True),
        preferred_element_type=jnp.float32,
    )
    up_val = jnp.dot(
        gathered, lax.all_gather(w_up, "sp", axis=0, tiled=True), preferred_element_type=jnp.float32
    )
    hidden = (jax.nn.silu(gate_val) * up_val).astype(jnp.bfloat16)
    partial_value = jnp.dot(
        hidden, lax.all_gather(w_down, "sp", axis=1, tiled=True), preferred_element_type=jnp.float32
    )
    ffn = lax.psum_scatter(
        partial_value.astype(jnp.bfloat16), "tp", scatter_dimension=0, tiled=True
    ).astype(jnp.float32)
    return (resid_mid + 0.5 * ffn).astype(jnp.bfloat16)


def solution(mesh):
    placed = (
        P(("sp", "tp"), None),
        P("sp", "tp"),
        P("tp", None),
        P("tp", None),
        P("sp", "tp"),
        P("tp", None, None),
        P("tp", None, None),
        P("tp", None, None),
        P("tp", None, None),
        P("tp", None),
        P(),
        P(),
        P(),
        P("sp", "tp"),
        P("sp", "tp"),
        P("tp", "sp"),
    )
    return jax.shard_map(
        per_device, mesh=mesh, in_specs=placed, out_specs=P(("sp", "tp"), None), check_vma=False
    )
```

profile of v0, /device:TPU:0, one launch (start us, length us, event | category | flops | bytes accessed | tf_op | source)
XLA Modules:
  0.0 576.9 jit_solution(734002597552785004)
XLA Ops:
  21.7 93.2 %while.45 = (s32[]{:T(128)}, f32[512]{0:T(512)S(1)}, f32[512]{0:T(512)S(1)}, f32[512]{0:T(512)S(1)}, f32[]{:T(128)}, /*index=5*/f32[8,32,512]{2,1,0:T(8,128)}, f...) while((s32[]{:T(128)}, f32[512]{0:T(512)S(1)}, ...), condition=%wide.wide.region_3.4_spmd.clone.clone.clone.clone, body=%wide.wide.region_0.3_spmd.clone.clone.clone.clone.sunk | while | flops 14897220 | bytes 1351775 | solution.py:78
  22.9 9.2 %add_reduce_fusion.3 = (f32[32,512]{1,0:T(8,128)S(1)}, f32[32,512]{1,0:T(8,128)S(1)}) fusion(f32[512]{0:T(512)S(1)} %get-tuple-element.853, f32[32,32]{1,0:T(8,128)S(1)} %get-tuple-element.854, f32[32,512]{1,0:T(8,128)S(1)} %get-tuple-element.788, f32[32,512]{1,0:T(8,128)S(1)} %get-tuple-element.789, ...), kind=kLoop, calls=%fused_computation.19.clone.clone.1 | loop fusion | flops 8355840 | bytes 335872 | tf_op jit(solution)/shard_map/while/body/eval_jaxpr/reduce_sum | solution.py:58
  34.5 9.2 %add_reduce_fusion.3 = (f32[32,512]{1,0:T(8,128)S(1)}, f32[32,512]{1,0:T(8,128)S(1)}) fusion(f32[512]{0:T(512)S(1)} %get-tuple-element.853, f32[32,32]{1,0:T(8,128)S(1)} %get-tuple-element.854, f32[32,512]{1,0:T(8,128)S(1)} %get-tuple-element.788, f32[32,512]{1,0:T(8,128)S(1)} %get-tuple-element.789, ...), kind=kLoop, calls=%fused_computation.19.clone.clone.1 | loop fusion | flops 8355840 | bytes 335872 | tf_op jit(solution)/shard_map/while/body/eval_jaxpr/reduce_sum | solution.py:58
  46.1 9.2 %add_reduce_fusion.3 = (f32[32,512]{1,0:T(8,128)S(1)}, f32[32,512]{1,0:T(8,128)S(1)}) fusion(f32[512]{0:T(512)S(1)} %get-tuple-element.853, f32[32,32]{1,0:T(8,128)S(1)} %get-tuple-element.854, f32[32,512]{1,0:T(8,128)S(1)} %get-tuple-element.788, f32[32,512]{1,0:T(8,128)S(1)} %get-tuple-element.789, ...), kind=kLoop, calls=%fused_computation.19.clone.clone.1 | loop fusion | flops 8355840 | bytes 335872 | tf_op jit(solution)/shard_map/while/body/eval_jaxpr/reduce_sum | solution.py:58
  57.8 9.2 %add_reduce_fusion.3 = (f32[32,512]{1,0:T(8,128)S(1)}, f32[32,512]{1,0:T(8,128)S(1)}) fusion(f32[512]{0:T(512)S(1)} %get-tuple-element.853, f32[32,32]{1,0:T(8,128)S(1)} %get-tuple-element.854, f32[32,512]{1,0:T(8,128)S(1)} %get-tuple-element.788, f32[32,512]{1,0:T(8,128)S(1)} %get-tuple-element.789, ...), kind=kLoop, calls=%fused_computation.19.clone.clone.1 | loop fusion | flops 8355840 | bytes 335872 | tf_op jit(solution)/shard_map/while/body/eval_jaxpr/reduce_sum | solution.py:58
  69.4 9.2 %add_reduce_fusion.3 = (f32[32,512]{1,0:T(8,128)S(1)}, f32[32,512]{1,0:T(8,128)S(1)}) fusion(f32[512]{0:T(512)S(1)} %get-tuple-element.853, f32[32,32]{1,0:T(8,128)S(1)} %get-tuple-element.854, f32[32,512]{1,0:T(8,128)S(1)} %get-tuple-element.788, f32[32,512]{1,0:T(8,128)S(1)} %get-tuple-element.789, ...), kind=kLoop, calls=%fused_computation.19.clone.clone.1 | loop fusion | flops 8355840 | bytes 335872 | tf_op jit(solution)/shard_map/while/body/eval_jaxpr/reduce_sum | solution.py:58
  81.1 9.2 %add_reduce_fusion.3 = (f32[32,512]{1,0:T(8,128)S(1)}, f32[32,512]{1,0:T(8,128)S(1)}) fusion(f32[512]{0:T(512)S(1)} %get-tuple-element.853, f32[32,32]{1,0:T(8,128)S(1)} %get-tuple-element.854, f32[32,512]{1,0:T(8,128)S(1)} %get-tuple-element.788, f32[32,512]{1,0:T(8,128)S(1)} %get-tuple-element.789, ...), kind=kLoop, calls=%fused_computation.19.clone.clone.1 | loop fusion | flops 8355840 | bytes 335872 | tf_op jit(solution)/shard_map/while/body/eval_jaxpr/reduce_sum | solution.py:58
  92.7 9.2 %add_reduce_fusion.3 = (f32[32,512]{1,0:T(8,128)S(1)}, f32[32,512]{1,0:T(8,128)S(1)}) fusion(f32[512]{0:T(512)S(1)} %get-tuple-element.853, f32[32,32]{1,0:T(8,128)S(1)} %get-tuple-element.854, f32[32,512]{1,0:T(8,128)S(1)} %get-tuple-element.788, f32[32,512]{1,0:T(8,128)S(1)} %get-tuple-element.789, ...), kind=kLoop, calls=%fused_computation.19.clone.clone.1 | loop fusion | flops 8355840 | bytes 335872 | tf_op jit(solution)/shard_map/while/body/eval_jaxpr/reduce_sum | solution.py:58
  104.4 9.2 %add_reduce_fusion.3 = (f32[32,512]{1,0:T(8,128)S(1)}, f32[32,512]{1,0:T(8,128)S(1)}) fusion(f32[512]{0:T(512)S(1)} %get-tuple-element.853, f32[32,32]{1,0:T(8,128)S(1)} %get-tuple-element.854, f32[32,512]{1,0:T(8,128)S(1)} %get-tuple-element.788, f32[32,512]{1,0:T(8,128)S(1)} %get-tuple-element.789, ...), kind=kLoop, calls=%fused_computation.19.clone.clone.1 | loop fusion | flops 8355840 | bytes 335872 | tf_op jit(solution)/shard_map/while/body/eval_jaxpr/reduce_sum | solution.py:58
  114.9 27.9 %all-gather.5 = f32[8,1,512]{2,1,0:T(1,128)S(1)} all-gather(f32[1,1,512]{2,1,0:T(1,128)S(1)} %bitcast.130), channel_id=3, replica_groups=mesh['sp'=8,'tp'=4] {'sp'}, dimensions={0}, use_global_device_ids=true | all-gather | bytes 18432 | tf_op jit(solution)/shard_map/all_gather | solution.py:11
  142.9 26.1 %all-gather.4 = f32[8,1,512]{2,1,0:T(1,128)S(1)} all-gather(f32[1,1,512]{2,1,0:T(1,128)S(1)} %bitcast.129), channel_id=2, replica_groups=mesh['sp'=8,'tp'=4] {'sp'}, dimensions={0}, use_global_device_ids=true | all-gather | bytes 18432 | tf_op jit(solution)/shard_map/all_gather | solution.py:11
  169.0 26.1 %all-gather.7 = f32[8,1,512]{2,1,0:T(1,128)S(1)} all-gather(f32[1,1,512]{2,1,0:T(1,128)S(1)} %bitcast.124), channel_id=5, replica_groups=mesh['sp'=8,'tp'=4] {'sp'}, dimensions={0}, use_global_device_ids=true | all-gather | bytes 18432 | tf_op jit(solution)/shard_map/all_gather | solution.py:11
  195.1 26.1 %all-gather.6 = f32[8,1,512]{2,1,0:T(1,128)S(1)} all-gather(f32[1,1,512]{2,1,0:T(1,128)S(1)} %bitcast.122), channel_id=4, replica_groups=mesh['sp'=8,'tp'=4] {'sp'}, dimensions={0}, use_global_device_ids=true | all-gather | bytes 18432 | tf_op jit(solution)/shard_map/all_gather | solution.py:11
  222.6 2.2 reshape.128
  224.9 2.2 reshape.129
  227.1 2.2 reshape.130
  234.1 6.7 %all_to_all.10 = bf16[4,64,128]{2,1,0:T(8,128)(2,1)S(1)} all-to-all(bf16[4,64,128]{2,1,0:T(8,128)(2,1)S(1)} %fusion.45), channel_id=1, replica_groups=mesh['sp'=8,'tp'=4] {'tp'}, dimensions={0} | all-to-all | bytes 131072 | tf_op jit(solution)/shard_map/all_to_all | solution.py:145
  244.7 10.7 %all-gather.13.cloned.1.call-done = bf16[256,2048]{1,0:T(8,128)(2,1)} async-done(((bf16[64,2048]{1,0:T(8,128)(2,1)}), bf16[256,2048]{1,0:T(8,128)(2,1)}) %all-gather.13.cloned.1.call-update) | async-done | bytes 1048592 | tf_op jit(solution)/shard_map/all_gather | solution.py:157
  255.5 94.5 %all-gather.15.cloned.1.call-done = bf16[2048,1408]{1,0:T(8,128)(2,1)} async-done(((bf16[256,1408]{1,0:T(8,128)(2,1)}), bf16[2048,1408]{1,0:T(8,128)(2,1)}) %all-gather.15.cloned.1.call-update) | async-done | bytes 5767184 | tf_op jit(solution)/shard_map/all_gather | solution.py:160
  350.0 5.9 %fusion.57 = f32[256,1408]{1,0:T(8,128)} fusion(bf16[256,2048]{1,0:T(8,128)(2,1)} %all-gather.13.cloned.1.call-done, bf16[2048,1408]{1,0:T(8,128)(2,1)} %all-gather.15.cloned.1.call-done), kind=kOutput, calls=%fused_computation.104 | convolution fusion | flops 1476395008 | bytes 8257536 | tf_op jit(solution)/shard_map/dot_general | solution.py:158
  355.9 86.8 %all-gather.17.cloned.1.call-done = bf16[2048,1408]{1,0:T(8,128)(2,1)} async-done(((bf16[256,1408]{1,0:T(8,128)(2,1)}), bf16[2048,1408]{1,0:T(8,128)(2,1)}) %all-gather.17.cloned.1.call-update) | async-done | bytes 5767184 | tf_op jit(solution)/shard_map/all_gather | solution.py:164
  442.7 93.2 %all-gather.19.cloned.1.call-done = bf16[1408,2048]{1,0:T(8,128)(2,1)} async-done(((bf16[1408,256]{1,0:T(8,128)(2,1)}), bf16[1408,2048]{1,0:T(8,128)(2,1)}) %all-gather.19.cloned.1.call-update) | async-done | bytes 5767184 | tf_op jit(solution)/shard_map/all_gather | solution.py:168
  536.0 9.5 %convolution_convert_fusion = bf16[256,2048]{1,0:T(8,128)(2,1)} fusion(bf16[1408,2048]{1,0:T(8,128)(2,1)} %all-gather.19.cloned.1.call-done, bf16[256,2048]{1,0:T(8,128)(2,1)} %all-gather.13.cloned.1.call-done, bf16[2048,1408]{1,0:T(8,128)(2,1)} %all-gather.17.cloned.1.call-done, f32[256,1408]{1,0:T(8,128)} %fusion.57), kind=kOutput, calls=%fused_computation.53 | convolution fusion | flops 2955476992 | bytes 15073280 | tf_op jit(solution)/shard_map/dot_general | solution.py:167
  545.5 23.1 %reduce-scatter.2.cloned.1.call-done = bf16[64,2048]{1,0:T(8,128)(2,1)} async-done(((bf16[256,2048]{1,0:T(8,128)(2,1)}), bf16[64,2048]{1,0:T(8,128)(2,1)}) %reduce-scatter.2.cloned.1.call-update) | async-done | bytes 262160 | tf_op jit(solution)/shard_map/reduce_scatter | solution.py:170
  (148 shorter events, 45.9 us)
Async XLA Ops:
  6.5 234.4 %copy-start = (bf16[512,2048]{1,0:T(8,128)(2,1)S(1)}, bf16[512,2048]{1,0:T(8,128)(2,1)}, u32[]{:S(2)}) copy-start(bf16[512,2048]{1,0:T(8,128)(2,1)} %param.31) | copy-start | bytes 6291460
  6.5 8.8 %copy-start.2 = (f32[8,64,16]{1,2,0:T(8,128)S(1)}, f32[8,64,16]{1,2,0:T(8,128)}, u32[]{:S(2)}) copy-start(f32[8,64,16]{1,2,0:T(8,128)} %param.26) | copy-start | bytes 98308
  6.5 249.0 %all-gather.13.cloned.1.call-start = ((), (), s32[]{:S(2)}) async-start(), calls=%async_computation.2 | async-start | bytes 1310720 | tf_op jit(solution)/shard_map/all_gather | solution.py:157
  15.3 3.7 copy-start.6
  229.3 2.2 copy-start.3
  229.3 3.3 copy-start.4
  229.3 3.3 copy-start.7
  231.5 9.4 %copy-start.1 = (bf16[64,2048]{1,0:T(8,128)(2,1)S(1)}, bf16[64,2048]{1,0:T(8,128)(2,1)}, u32[]{:S(2)}) copy-start(bf16[64,2048]{1,0:T(8,128)(2,1)} %param.20) | copy-start | bytes 786436
  231.5 9.4 %copy-start.8 = (f32[512]{0:T(512)S(1)}, f32[512]{0:T(512)}, u32[]{:S(2)}) copy-start(f32[512]{0:T(512)} %param.30) | copy-start | bytes 6148
  233.8 7.8 %copy-start.5 = (f32[2048]{0:T(1024)S(1)}, f32[2048]{0:T(1024)}, u32[]{:S(2)}) copy-start(f32[2048]{0:T(1024)} %param.32) | copy-start | bytes 24580
  242.5 107.6 %all-gather.15.cloned.1.call-start = ((), (), s32[]{:S(2)}) async-start(), calls=%async_computation.3 | async-start | bytes 6488064 | tf_op jit(solution)/shard_map/all_gather | solution.py:160
  243.2 199.5 %all-gather.17.cloned.1.call-start = ((), (), s32[]{:S(2)}) async-start(), calls=%async_computation.4 | async-start | bytes 6488064 | tf_op jit(solution)/shard_map/all_gather | solution.py:164
  243.9 292.0 %all-gather.19.cloned.1.call-start = ((), (), s32[]{:S(2)}) async-start(), calls=%async_computation.5 | async-start | bytes 6488064 | tf_op jit(solution)/shard_map/all_gather | solution.py:168
  244.5 324.1 %reduce-scatter.2.cloned.1.call-start = ((), (), s32[]{:S(2)}) async-start(), calls=%async_computation.6 | async-start | bytes 1310720 | tf_op jit(solution)/shard_map/reduce_scatter | solution.py:170
Sparse Core Ops, SparseCore 0:
  242.6 12.8 all-gather.12
  257.7 92.3 all-gather.14
  352.2 90.4 all-gather.16
  444.6 91.2 all-gather.18
  545.6 22.9 reduce-scatter.1
where the time goes:
time: 578 us; the launch traced here: 577 us
  waiting for transfers between devices  310 us (54%)
  blocking collectives  113 us (20%)
  other arithmetic  90.7 us (16%)
  local copies, waits for them, and re-layouts  25.5 us (4%)
  matrix products  23.1 us (4%)
  between operations  13.3 us (2%)
    all_gather x4, blocking collectives, carried_in(): gathered = jax.tree.map(lambda a: lax.all_gather(a, axis), part)  106 us
    all_gather x1, waiting for transfers between devices, per_device(): lax.all_gather(gating_matrix, 'sp', axis=0, tiled=True)  94.5 us
    all_gather x1, waiting for transfers between devices, per_device(): lax.all_gather(w_down, 'sp', axis=1, tiled=True)  93.2 us
    all_gather x1, waiting for transfers between devices, per_device(): lax.all_gather(w_up, 'sp', axis=0, tiled=True)  86.8 us
    reduce_sum x8, other arithmetic, advance(): jnp.sum(weight_real * imag_block[None] + weight_imag * real_block[None],...  73.6 us
    reduce_scatter x1, waiting for transfers between devices, per_device(): lax.psum_scatter(partial_value.astype(jnp.bfloat16), 'tp', scatter_dimens...  23.1 us
  transfers between devices with their start and end apart: 5, of which 5 were waited for; matrix products, arithmetic and copies ran while one was open for 1% of the time, Pallas kernels for 0%

commit v1 on v0

--- a/solution.py
+++ b/solution.py
@@ -165,7 +165,9 @@
     )
     hidden = (jax.nn.silu(gate_val) * up_val).astype(jnp.bfloat16)
     partial_value = jnp.dot(
-        hidden, lax.all_gather(w_down, "sp", axis=1, tiled=True), preferred_element_type=jnp.float32
+        hidden,
+        jnp.concatenate(lax.all_gather(w_down, "sp"), axis=1),
+        preferred_element_type=jnp.float32,
     )
     ffn = lax.psum_scatter(
         partial_value.astype(jnp.bfloat16), "tp", scatter_dimension=0, tiled=True

time: 578 us -> 486 us (0.84)
  waiting for transfers between devices: 310 us -> 209 us
  local copies, waits for them, and re-layouts: 25.5 us -> 34 us
    all_gather x1, waiting for transfers between devices: 93.2 us -> 0.02 us  [per_device(): lax.all_gather(w_down, 'sp')]
    reshape x0 -> x1, local copies, waits for them, and re-layouts: none -> 8.4 us  [per_device(): jnp.concatenate(lax.all_gather(w_down, 'sp'), axis=1)]
    all_gather x1, waiting for transfers between devices: 10.7 us -> 3.06 us  [per_device(): gathered = lax.all_gather(ffn_in, 'tp', axis=0, tiled=True)]
  transfers between devices with their start and end apart: 5 -> 5, of which waited for: 5 -> 4; matrix products, arithmetic and copies ran while one was open for 1% -> 28% of each run, Pallas kernels for 0% -> 0%
where the time goes in v1:
time: 486 us; the launch traced here: 484 us
  waiting for transfers between devices  209 us (43%)
  blocking collectives  113 us (23%)
  other arithmetic  90.6 us (19%)
  local copies, waits for them, and re-layouts  34 us (7%)
  matrix products  23.2 us (5%)
  between operations  13.4 us (3%)
    all_gather x4, blocking collectives, carried_in(): gathered = jax.tree.map(lambda a: lax.all_gather(a, axis), part)  106 us
    all_gather x1, waiting for transfers between devices, per_device(): lax.all_gather(gating_matrix, 'sp', axis=0, tiled=True)  94.5 us
    all_gather x1, waiting for transfers between devices, per_device(): lax.all_gather(w_up, 'sp', axis=0, tiled=True)  86.7 us
    reduce_sum x8, other arithmetic, advance(): jnp.sum(weight_real * imag_block[None] + weight_imag * real_block[None],...  73.6 us
    reduce_scatter x1, waiting for transfers between devices, per_device(): lax.psum_scatter(partial_value.astype(jnp.bfloat16), 'tp', scatter_dimens...  23.1 us
    dynamic_update_slice x8, other arithmetic, local_states(): final, outputs = lax.scan(advance, start, blocks)  9.94 us
  transfers between devices with their start and end apart: 5, of which 4 were waited for; matrix products, arithmetic and copies ran while one was open for 28% of the time, Pallas kernels for 0%

profile of v1, /device:TPU:0, one launch (start us, length us, event | category | flops | bytes accessed | tf_op | source)
XLA Modules:
  0.0 484.3 jit_solution(6662259509079659011)
XLA Ops:
  22.5 93.2 %while.45 = (s32[]{:T(128)}, f32[512]{0:T(512)S(1)}, f32[512]{0:T(512)S(1)}, f32[512]{0:T(512)S(1)}, f32[]{:T(128)}, /*index=5*/f32[8,32,512]{2,1,0:T(8,128)}, f...) while((s32[]{:T(128)}, f32[512]{0:T(512)S(1)}, ...), condition=%wide.wide.region_3.4_spmd.clone.clone.clone.clone, body=%wide.wide.region_0.3_spmd.clone.clone.clone.clone.sunk | while | flops 14897220 | bytes 1351775 | solution.py:78
  23.6 9.2 %add_reduce_fusion.3 = (f32[32,512]{1,0:T(8,128)S(1)}, f32[32,512]{1,0:T(8,128)S(1)}) fusion(f32[512]{0:T(512)S(1)} %get-tuple-element.853, f32[32,32]{1,0:T(8,128)S(1)} %get-tuple-element.854, f32[32,512]{1,0:T(8,128)S(1)} %get-tuple-element.788, f32[32,512]{1,0:T(8,128)S(1)} %get-tuple-element.789, ...), kind=kLoop, calls=%fused_computation.19.clone.clone.1 | loop fusion | flops 8355840 | bytes 335872 | tf_op jit(solution)/shard_map/while/body/eval_jaxpr/reduce_sum | solution.py:58
  35.3 9.2 %add_reduce_fusion.3 = (f32[32,512]{1,0:T(8,128)S(1)}, f32[32,512]{1,0:T(8,128)S(1)}) fusion(f32[512]{0:T(512)S(1)} %get-tuple-element.853, f32[32,32]{1,0:T(8,128)S(1)} %get-tuple-element.854, f32[32,512]{1,0:T(8,128)S(1)} %get-tuple-element.788, f32[32,512]{1,0:T(8,128)S(1)} %get-tuple-element.789, ...), kind=kLoop, calls=%fused_computation.19.clone.clone.1 | loop fusion | flops 8355840 | bytes 335872 | tf_op jit(solution)/shard_map/while/body/eval_jaxpr/reduce_sum | solution.py:58
  46.9 9.2 %add_reduce_fusion.3 = (f32[32,512]{1,0:T(8,128)S(1)}, f32[32,512]{1,0:T(8,128)S(1)}) fusion(f32[512]{0:T(512)S(1)} %get-tuple-element.853, f32[32,32]{1,0:T(8,128)S(1)} %get-tuple-element.854, f32[32,512]{1,0:T(8,128)S(1)} %get-tuple-element.788, f32[32,512]{1,0:T(8,128)S(1)} %get-tuple-element.789, ...), kind=kLoop, calls=%fused_computation.19.clone.clone.1 | loop fusion | flops 8355840 | bytes 335872 | tf_op jit(solution)/shard_map/while/body/eval_jaxpr/reduce_sum | solution.py:58
  58.6 9.2 %add_reduce_fusion.3 = (f32[32,512]{1,0:T(8,128)S(1)}, f32[32,512]{1,0:T(8,128)S(1)}) fusion(f32[512]{0:T(512)S(1)} %get-tuple-element.853, f32[32,32]{1,0:T(8,128)S(1)} %get-tuple-element.854, f32[32,512]{1,0:T(8,128)S(1)} %get-tuple-element.788, f32[32,512]{1,0:T(8,128)S(1)} %get-tuple-element.789, ...), kind=kLoop, calls=%fused_computation.19.clone.clone.1 | loop fusion | flops 8355840 | bytes 335872 | tf_op jit(solution)/shard_map/while/body/eval_jaxpr/reduce_sum | solution.py:58
  70.2 9.2 %add_reduce_fusion.3 = (f32[32,512]{1,0:T(8,128)S(1)}, f32[32,512]{1,0:T(8,128)S(1)}) fusion(f32[512]{0:T(512)S(1)} %get-tuple-element.853, f32[32,32]{1,0:T(8,128)S(1)} %get-tuple-element.854, f32[32,512]{1,0:T(8,128)S(1)} %get-tuple-element.788, f32[32,512]{1,0:T(8,128)S(1)} %get-tuple-element.789, ...), kind=kLoop, calls=%fused_computation.19.clone.clone.1 | loop fusion | flops 8355840 | bytes 335872 | tf_op jit(solution)/shard_map/while/body/eval_jaxpr/reduce_sum | solution.py:58
  81.9 9.2 %add_reduce_fusion.3 = (f32[32,512]{1,0:T(8,128)S(1)}, f32[32,512]{1,0:T(8,128)S(1)}) fusion(f32[512]{0:T(512)S(1)} %get-tuple-element.853, f32[32,32]{1,0:T(8,128)S(1)} %get-tuple-element.854, f32[32,512]{1,0:T(8,128)S(1)} %get-tuple-element.788, f32[32,512]{1,0:T(8,128)S(1)} %get-tuple-element.789, ...), kind=kLoop, calls=%fused_computation.19.clone.clone.1 | loop fusion | flops 8355840 | bytes 335872 | tf_op jit(solution)/shard_map/while/body/eval_jaxpr/reduce_sum | solution.py:58
  93.5 9.2 %add_reduce_fusion.3 = (f32[32,512]{1,0:T(8,128)S(1)}, f32[32,512]{1,0:T(8,128)S(1)}) fusion(f32[512]{0:T(512)S(1)} %get-tuple-element.853, f32[32,32]{1,0:T(8,128)S(1)} %get-tuple-element.854, f32[32,512]{1,0:T(8,128)S(1)} %get-tuple-element.788, f32[32,512]{1,0:T(8,128)S(1)} %get-tuple-element.789, ...), kind=kLoop, calls=%fused_computation.19.clone.clone.1 | loop fusion | flops 8355840 | bytes 335872 | tf_op jit(solution)/shard_map/while/body/eval_jaxpr/reduce_sum | solution.py:58
  105.2 9.2 %add_reduce_fusion.3 = (f32[32,512]{1,0:T(8,128)S(1)}, f32[32,512]{1,0:T(8,128)S(1)}) fusion(f32[512]{0:T(512)S(1)} %get-tuple-element.853, f32[32,32]{1,0:T(8,128)S(1)} %get-tuple-element.854, f32[32,512]{1,0:T(8,128)S(1)} %get-tuple-element.788, f32[32,512]{1,0:T(8,128)S(1)} %get-tuple-element.789, ...), kind=kLoop, calls=%fused_computation.19.clone.clone.1 | loop fusion | flops 8355840 | bytes 335872 | tf_op jit(solution)/shard_map/while/body/eval_jaxpr/reduce_sum | solution.py:58
  115.7 27.9 %all-gather.6 = f32[8,1,512]{2,1,0:T(1,128)S(1)} all-gather(f32[1,1,512]{2,1,0:T(1,128)S(1)} %bitcast.136), channel_id=3, replica_groups=mesh['sp'=8,'tp'=4] {'sp'}, dimensions={0}, use_global_device_ids=true | all-gather | bytes 18432 | tf_op jit(solution)/shard_map/all_gather | solution.py:11
  143.7 26.1 %all-gather.5 = f32[8,1,512]{2,1,0:T(1,128)S(1)} all-gather(f32[1,1,512]{2,1,0:T(1,128)S(1)} %bitcast.135), channel_id=2, replica_groups=mesh['sp'=8,'tp'=4] {'sp'}, dimensions={0}, use_global_device_ids=true | all-gather | bytes 18432 | tf_op jit(solution)/shard_map/all_gather | solution.py:11
  169.8 26.1 %all-gather.8 = f32[8,1,512]{2,1,0:T(1,128)S(1)} all-gather(f32[1,1,512]{2,1,0:T(1,128)S(1)} %bitcast.130), channel_id=5, replica_groups=mesh['sp'=8,'tp'=4] {'sp'}, dimensions={0}, use_global_device_ids=true | all-gather | bytes 18432 | tf_op jit(solution)/shard_map/all_gather | solution.py:11
  195.9 26.1 %all-gather.7 = f32[8,1,512]{2,1,0:T(1,128)S(1)} all-gather(f32[1,1,512]{2,1,0:T(1,128)S(1)} %bitcast.128), channel_id=4, replica_groups=mesh['sp'=8,'tp'=4] {'sp'}, dimensions={0}, use_global_device_ids=true | all-gather | bytes 18432 | tf_op jit(solution)/shard_map/all_gather | solution.py:11
  223.4 2.2 reshape.134
  225.7 2.2 reshape.135
  227.9 2.3 reshape.136
  235.0 6.7 %all_to_all.10 = bf16[4,64,128]{2,1,0:T(8,128)(2,1)S(1)} all-to-all(bf16[4,64,128]{2,1,0:T(8,128)(2,1)S(1)} %fusion.45), channel_id=1, replica_groups=mesh['sp'=8,'tp'=4] {'tp'}, dimensions={0} | all-to-all | bytes 131072 | tf_op jit(solution)/shard_map/all_to_all | solution.py:145
  244.9 8.4 %copy.72 = bf16[1408,8,256]{0,2,1:T(8,128)(2,1)} copy(bf16[1408,8,256]{2,0,1:T(8,128)(2,1)} %bitcast.117) | data formatting | bytes 11534336 | tf_op jit(solution)/shard_map/reshape | solution.py:169
  253.3 3.1 all-gather.14.cloned.1.call-done
  256.3 94.5 %all-gather.16.cloned.1.call-done = bf16[2048,1408]{1,0:T(8,128)(2,1)} async-done(((bf16[256,1408]{1,0:T(8,128)(2,1)}), bf16[2048,1408]{1,0:T(8,128)(2,1)}) %all-gather.16.cloned.1.call-update) | async-done | bytes 5767184 | tf_op jit(solution)/shard_map/all_gather | solution.py:160
  350.9 5.9 %fusion.57 = f32[256,1408]{1,0:T(8,128)} fusion(bf16[256,2048]{1,0:T(8,128)(2,1)} %all-gather.14.cloned.1.call-done, bf16[2048,1408]{1,0:T(8,128)(2,1)} %all-gather.16.cloned.1.call-done), kind=kOutput, calls=%fused_computation.104 | convolution fusion | flops 1476395008 | bytes 8257536 | tf_op jit(solution)/shard_map/dot_general | solution.py:158
  356.8 86.7 %all-gather.18.cloned.1.call-done = bf16[2048,1408]{1,0:T(8,128)(2,1)} async-done(((bf16[256,1408]{1,0:T(8,128)(2,1)}), bf16[2048,1408]{1,0:T(8,128)(2,1)}) %all-gather.18.cloned.1.call-update) | async-done | bytes 5767184 | tf_op jit(solution)/shard_map/all_gather | solution.py:164
  443.4 9.5 %convolution_convert_fusion = bf16[256,2048]{1,0:T(8,128)(2,1)} fusion(bf16[1408,2048]{0,1:T(8,128)(2,1)} %bitcast.118, bf16[256,2048]{1,0:T(8,128)(2,1)} %all-gather.14.cloned.1.call-done, bf16[2048,1408]{1,0:T(8,128)(2,1)} %all-gather.18.cloned.1.call-done, f32[256,1408]{1,0:T(8,128)} %fusion.57), kind=kOutput, calls=%fused_computation.53 | convolution fusion | flops 2955476992 | bytes 15073280 | tf_op jit(solution)/shard_map/dot_general | solution.py:167
  452.9 23.1 %reduce-scatter.2.cloned.1.call-done = bf16[64,2048]{1,0:T(8,128)(2,1)} async-done(((bf16[256,2048]{1,0:T(8,128)(2,1)}), bf16[64,2048]{1,0:T(8,128)(2,1)}) %reduce-scatter.2.cloned.1.call-update) | async-done | bytes 262160 | tf_op jit(solution)/shard_map/reduce_scatter | solution.py:172
  (149 shorter events, 46.0 us)
Async XLA Ops:
  6.5 235.2 %copy-start = (bf16[512,2048]{1,0:T(8,128)(2,1)S(1)}, bf16[512,2048]{1,0:T(8,128)(2,1)}, u32[]{:S(2)}) copy-start(bf16[512,2048]{1,0:T(8,128)(2,1)} %param.31) | copy-start | bytes 6291460
  6.5 238.3 %all-gather.20.cloned.1.call-start = ((), (), s32[]{:S(2)}) async-start(), calls=%async_computation.6 | async-start | bytes 6488064 | tf_op jit(solution)/shard_map/all_gather | solution.py:169
  7.3 8.7 %copy-start.2 = (f32[8,64,16]{1,2,0:T(8,128)S(1)}, f32[8,64,16]{1,2,0:T(8,128)}, u32[]{:S(2)}) copy-start(f32[8,64,16]{1,2,0:T(8,128)} %param.26) | copy-start | bytes 98308
  7.3 249.1 %all-gather.14.cloned.1.call-start = ((), (), s32[]{:S(2)}) async-start(), calls=%async_computation.2 | async-start | bytes 1310720 | tf_op jit(solution)/shard_map/all_gather | solution.py:157
  16.0 3.7 copy-start.6
  230.2 2.2 copy-start.3
  230.2 3.3 copy-start.4
  230.2 3.3 copy-start.7
  232.3 9.4 %copy-start.1 = (bf16[64,2048]{1,0:T(8,128)(2,1)S(1)}, bf16[64,2048]{1,0:T(8,128)(2,1)}, u32[]{:S(2)}) copy-start(bf16[64,2048]{1,0:T(8,128)(2,1)} %param.20) | copy-start | bytes 786436
  232.4 9.4 %copy-start.8 = (f32[512]{0:T(512)S(1)}, f32[512]{0:T(512)}, u32[]{:S(2)}) copy-start(f32[512]{0:T(512)} %param.30) | copy-start | bytes 6148
  234.6 7.8 %copy-start.5 = (f32[2048]{0:T(1024)S(1)}, f32[2048]{0:T(1024)}, u32[]{:S(2)}) copy-start(f32[2048]{0:T(1024)} %param.32) | copy-start | bytes 24580
  243.3 107.6 %all-gather.16.cloned.1.call-start = ((), (), s32[]{:S(2)}) async-start(), calls=%async_computation.3 | async-start | bytes 6488064 | tf_op jit(solution)/shard_map/all_gather | solution.py:160
  244.0 199.4 %all-gather.18.cloned.1.call-start = ((), (), s32[]{:S(2)}) async-start(), calls=%async_computation.4 | async-start | bytes 6488064 | tf_op jit(solution)/shard_map/all_gather | solution.py:164
  244.6 231.4 %reduce-scatter.2.cloned.1.call-start = ((), (), s32[]{:S(2)}) async-start(), calls=%async_computation.5 | async-start | bytes 1310720 | tf_op jit(solution)/shard_map/reduce_scatter | solution.py:172
Sparse Core Ops, SparseCore 0:
  9.5 95.0 all-gather.19
  243.4 12.8 all-gather.13
  258.5 92.3 all-gather.15
  352.9 90.4 all-gather.17
  453.1 22.9 reduce-scatter.1
